TPU v7x, 32 devices: a whole 2x2x4 slice. The times are simulated.
32 devices in a mesh: ep: 8 (over z, y), tp: 4 (over x, core).
Axes of the slice: x: 2, y: 2, z: 4, core: 2. Of those that a mesh axis runs over, the one named last changes fastest.
Arguments:
- queries: bfloat16 [4096, 1024], P('ep', 'tp'), may hold values from -6 to 6
- keys: bfloat16 [4096, 512], P('ep', 'tp'), may hold values from -6 to 6
- values: bfloat16 [4096, 512], P('ep', 'tp'), may hold values from -6 to 6
- forget_cache: float32 [8, 4096], P('tp'), may hold values from -412 to 0, as said below
- query_gain: float32 [128], replicated, may hold values from 0.6 to 6
- key_gain: float32 [128], replicated, may hold values from 0.6 to 6
- mixer_out: bfloat16 [1024, 2048], replicated, may hold values from -0.75 to 0.75
- expert_input: bfloat16 [4096, 2048], P(('ep', 'tp')), may hold values from -6 to 6
- norm_gain: float32 [2048], replicated, may hold values from 0.1 to 1.9
- routes: int32 [4096, 2], P(('ep', 'tp')), may hold values from 0 to 31, all different within a row; in each aligned block of 128 rows (0 to 127, 128 to 255, ...) at most 16 rows name the same one
- route_weights: float32 [4096, 2], P(('ep', 'tp')), may hold values from 0.1 to 1
- w_gate: bfloat16 [32, 2048, 1024], P('ep', None, 'tp'), may hold values from -0.125 to 0.125
- w_up: bfloat16 [32, 2048, 1024], P('ep', None, 'tp'), may hold values from -0.125 to 0.125
- w_down: bfloat16 [32, 2048, 1024], P('ep', None, 'tp'), may hold values from -0.1875 to 0.1875
Outputs:
- mixed: bfloat16 [4096, 2048], P(('ep', 'tp'))
- routed: bfloat16 [4096, 2048], P(('ep', 'tp'))
Inputs may be any that keep to these rules, and one draw needn't show every extreme that they name: `routes`: each row names 2 different experts; among the rows of one device no expert is named by more than 16 rows, a bound that some block reaches. `forget_cache`: never rises along the positions.
All inputs are finite; a program needn't handle non-finite values.
Results may differ from a plain program's by a relative error of at most 0.013.
The roundings to bfloat16 on the way count: a program that leaves them out, or rounds other values in their place, can miss the bound.
Values may be sent and summed in bfloat16 or wider, within the bound.
A program may use at most 128 MiB of HBM per device.

v0:
```python
import math

import jax
import jax.numpy as jnp
from jax import lax
from jax.sharding import PartitionSpec as P

EXPERTS = 32
CAP = 16


EPSILON = 1e-06
NEGATIVE = -1e30


def rms_scale(inputs, gain):
    inputs = inputs.astype(jnp.float32)
    return inputs * lax.rsqrt(jnp.mean(inputs * inputs, axis=-1, keepdims=True) + EPSILON) * gain


def attend(queries, keys, values, forget_cache, query_gain, key_gain):
    rows = queries.shape[0]
    head_dim = keys.shape[1]
    local_heads = forget_cache.shape[0]
    first = lax.axis_index("ep") * rows
    normed_q = rms_scale(queries.reshape(rows, local_heads, head_dim), query_gain).astype(
        jnp.bfloat16
    )
    normed_k = rms_scale(keys, key_gain).astype(jnp.bfloat16)
    scale = head_dim ** (-0.5)
    groups = [(normed_q, first + jnp.arange(rows, dtype=jnp.int32))]
    gate_sets = [jnp.take(forget_cache, position, axis=1) for _, position in groups]
    initial = tuple(
        (
            (
                jnp.full((local_heads, group_rows.shape[0]), NEGATIVE, jnp.float32),
                jnp.zeros((local_heads, group_rows.shape[0]), jnp.float32),
                jnp.zeros((local_heads, group_rows.shape[0], head_dim), jnp.float32),
            )
            for group_rows, _ in groups
        )
    )
    key_matrix_rows = lax.all_gather(normed_k, "ep", axis=0, tiled=True)
    value_rows = lax.all_gather(values, "ep", axis=0, tiled=True)
    length = key_matrix_rows.shape[0]
    width = math.gcd(length, 512)
    query_rows, query_pos = groups[0]
    query_gates = gate_sets[0]
    last_pos = jnp.max(query_pos)

    def one_block(number, inner):
        begin = number * width

        def update(current):
            highest, denom, accum = current
            block_keys = lax.dynamic_slice_in_dim(key_matrix_rows, number * width, width, 0)
            block_values = lax.dynamic_slice_in_dim(value_rows, number * width, width, 0)
            key_gates = lax.dynamic_slice_in_dim(forget_cache, begin, width, 1)
            scores = (
                jnp.einsum(
                    "qhd,kd->hqk", query_rows, block_keys, preferred_element_type=jnp.float32
                )
                * scale
            )
            scores = scores + query_gates[:, :, None] - key_gates[:, None, :]
            key_pos = begin + jnp.arange(width, dtype=jnp.int32)
            allowed = key_pos[None, :] <= query_pos[:, None]
            scores = jnp.where(allowed[None], scores, NEGATIVE)
            newest = jnp.maximum(highest, jnp.max(scores, axis=2))
            weights = jnp.where(allowed[None], jnp.exp(scores - newest[:, :, None]), 0.0)
            factor = jnp.exp(highest - newest)
            denom = denom * factor + jnp.sum(weights, axis=2)
            product = jnp.einsum(
                "hqk,kd->hqd",
                weights.astype(jnp.bfloat16),
                block_values,
                preferred_element_type=jnp.float32,
            )
            accum = accum * factor[:, :, None] + product
            return (newest, denom, accum)

        return lax.cond(begin <= last_pos, update, lambda current: current, inner)

    results = [lax.fori_loop(0, length // width, one_block, initial[0])]
    finals = tuple(results)
    outputs = [(accum / denom[:, :, None]).astype(jnp.bfloat16) for _, denom, accum in finals]
    return outputs[0]


def dispatch(expert_input, norm_gain, routes):
    rows = expert_input.shape[0]
    top = routes.shape[1]
    normed = rms_scale(expert_input, norm_gain).astype(jnp.bfloat16)
    flat = routes.reshape(-1)
    onehot = (flat[:, None] == jnp.arange(EXPERTS, dtype=jnp.int32)[None, :]).astype(jnp.int32)
    prior_state = jnp.cumsum(onehot, axis=0) - onehot
    rank = jnp.sum(prior_state * onehot, axis=1)
    slots = rank * EXPERTS + flat
    owner = (
        jnp.full((CAP * EXPERTS,), rows, jnp.int32)
        .at[slots]
        .set(jnp.arange(rows * top, dtype=jnp.int32) // top)
    )
    padded = jnp.concatenate([normed, jnp.zeros((1, normed.shape[1]), jnp.bfloat16)], axis=0)
    outgoing = padded[owner].reshape(CAP, EXPERTS, normed.shape[1])
    received = lax.all_to_all(outgoing, "ep", split_axis=1, concat_axis=0, tiled=True)
    return (received, slots)


def on_device(
    queries,
    keys,
    values,
    forget_cache,
    query_gain,
    key_gain,
    mixer_out,
    expert_input,
    norm_gain,
    routes,
    route_weights,
    w_gate,
    w_up,
    w_down,
):
    attended = attend(queries, keys, values, forget_cache, query_gain, key_gain)
    received, slots = dispatch(expert_input, norm_gain, routes)
    regrouped = lax.all_to_all(attended, "tp", split_axis=1, concat_axis=0, tiled=True)
    all_heads = regrouped.shape[0]
    projection = mixer_out.reshape(all_heads, regrouped.shape[2], mixer_out.shape[1])
    mixed = jnp.einsum(
        "hqd,hde->qe", regrouped, projection, preferred_element_type=jnp.float32
    ).astype(jnp.bfloat16)
    pieces = lax.all_gather(received, "tp", axis=0, tiled=True)
    gate = jnp.einsum("red,edf->ref", pieces, w_gate, preferred_element_type=jnp.float32)
    upward = jnp.einsum("red,edf->ref", pieces, w_up, preferred_element_type=jnp.float32)
    hidden = (jax.nn.silu(gate) * upward).astype(jnp.bfloat16)
    summed = lax.psum_scatter(
        jnp.einsum("ref,edf->red", hidden, w_down, preferred_element_type=jnp.float32).astype(
            jnp.bfloat16
        ),
        "tp",
        scatter_dimension=0,
        tiled=True,
    )
    returned = lax.all_to_all(summed, "ep", split_axis=0, concat_axis=1, tiled=True)
    flat_back = returned.reshape(-1, returned.shape[2])
    picked = (
        flat_back[slots]
        .reshape(routes.shape[0], routes.shape[1], returned.shape[2])
        .astype(jnp.float32)
    )
    routed = jnp.sum(picked * route_weights[:, :, None], axis=1).astype(jnp.bfloat16)
    return (mixed, routed)


def solution(mesh):
    in_specs = (
        P("ep", "tp"),
        P("ep", "tp"),
        P("ep", "tp"),
        P("tp", None),
        P(),
        P(),
        P(),
        P(("ep", "tp"), None),
        P(),
        P(("ep", "tp"), None),
        P(("ep", "tp"), None),
        P("ep", None, "tp"),
        P("ep", None, "tp"),
        P("ep", None, "tp"),
    )
    out_specs = (P(("ep", "tp"), None), P(("ep", "tp"), None))
    return jax.shard_map(
        on_device, mesh=mesh, in_specs=in_specs, out_specs=out_specs, check_vma=False
    )
```

profile of v0, /device:TPU:16, one launch (start us, length us, event | category | flops | bytes accessed | tf_op | source)
XLA Modules:
  0.0 362.9 jit_solution(14982361686460898123)
XLA Ops:
  7.2 0.8 copy.60
  9.4 1.4 scatter_custom_fusion
  10.8 1.2 fusion.22
  12.1 1.2 fusion.24
  13.4 2.5 gather_fusion.1
  15.8 1.2 copy.64
  17.0 52.3 %all_to_all.51 = bf16[16,32,2048]{2,0,1:T(8,128)(2,1)S(1)} all-to-all(bf16[16,32,2048]{2,0,1:T(8,128)(2,1)S(1)} %copy.64), channel_id=1, replica_groups=mesh['ep'=8,'tp'=4] {'ep'}, dimensions={1} | all-to-all | bytes 4194304 | tf_op jit(solution)/shard_map/all_to_all | solution.py:106
  69.3 1.5 copy.65
  70.9 0.8 copy-done
  71.9 0.8 fusion.30
  72.8 0.7 all-gather.6.cloned.1.call-update
  73.7 55.9 %all-gather.8.cloned.1.call-done = bf16[512,4,2048]{2,0,1:T(8,128)(2,1)} async-done(((bf16[128,4,2048]{2,0,1:T(8,128)(2,1)}), bf16[512,4,2048]{2,0,1:T(8,128)(2,1)}) %all-gather.8.cloned.1.call-update) | async-done | bytes 8388624 | tf_op jit(solution)/shard_map/all_gather | solution.py:134
  129.6 6.9 %fusion.42 = f32[4,512,256]{2,1,0:T(8,128)S(1)} fusion(bf16[512,4,2048]{2,0,1:T(8,128)(2,1)} %all-gather.8.cloned.1.call-done, bf16[4,2048,256]{2,1,0:T(8,128)(2,1)} %param.29), kind=kOutput, calls=%fused_computation.89 | convolution fusion | flops 2147483648 | bytes 14680064 | tf_op jit(solution)/shard_map/red,edf->ref/dot_general | solution.py:135
  136.5 14.0 %convert_bitcast_fusion = bf16[512,4,2048]{2,0,1:T(8,128)(2,1)} fusion(bf16[4,2048,256]{2,1,0:T(8,128)(2,1)} %param.31, f32[4,512,256]{2,1,0:T(8,128)S(1)} %fusion.42, bf16[512,4,2048]{2,0,1:T(8,128)(2,1)} %all-gather.8.cloned.1.call-done, bf16[4,2048,256]{2,1,0:T(8,128)(2,1)} %param.30), kind=kOutput, calls=%fused_computation.28 | convolution fusion | flops 4302307328 | bytes 27262976 | tf_op jit(solution)/shard_map/ref,edf->red/dot_general | solution.py:139
  150.6 0.7 copy-done.2
  151.3 0.6 copy.55
  151.9 0.6 fusion.35
  152.6 1.0 gather_fusion
  154.4 16.4 %all-gather.4.cloned.1.call-done = bf16[4096,128]{1,0:T(8,128)(2,1)} async-done(((bf16[512,128]{1,0:T(8,128)(2,1)}), bf16[4096,128]{1,0:T(8,128)(2,1)}) %all-gather.4.cloned.1.call-update) | async-done | bytes 1048592 | tf_op jit(solution)/shard_map/all_gather | solution.py:43
  170.8 41.2 %all-gather.6.cloned.1.call-done = bf16[4096,128]{1,0:T(8,128)(2,1)} async-done(((bf16[512,128]{1,0:T(8,128)(2,1)}), bf16[4096,128]{1,0:T(8,128)(2,1)}) %all-gather.6.cloned.1.call-update) | async-done | bytes 1048592 | tf_op jit(solution)/shard_map/all_gather | solution.py:44
  212.1 25.0 %while.18 = (s32[]{:T(128)}, f32[2,512]{1,0:T(2,128)S(1)}, f32[2,512]{1,0:T(2,128)S(1)}, f32[2,512,128]{2,1,0:T(8,128)S(1)}, s32[]{:T(128)}, /*index=5*/bf16[409...) while((s32[]{:T(128)}, f32[2,512]{1,0:T(2,128)S(1)}, ...), condition=%wide.region_8.9_spmd.clone, body=%wide.region_3.8_spmd.clone.sunk | while | flops 274729984 | bytes 9007507 | solution.py:84
  212.6 4.0 %conditional.3 = ((f32[2,512]{1,0:T(2,128)S(1)}, f32[2,512]{1,0:T(2,128)S(1)}, f32[2,512,128]{2,1,0:T(8,128)S(1)})) conditional(s32[]{:T(128)} %convert_element_type.114, (f32[2,512]{1,0:T(2,128)S(1)}, f32[2,512]{1,0:T(2,128)S(1)}, f32[2,512,128]{2,1,0:T(8,128)S(1)}) %tuple.53, (s32[]{:T(128)}, s32[]{:T(128)}, s32[]{:T(128)}, ...), branch_computations={%region_4.4_spmd, %region_5.0_spmd} | conditional | flops 274729984 | bytes 9005188 | solution.py:82
  212.9 1.6 fusion.41
  215.0 1.7 convolution_add_fusion
  217.2 4.1 %conditional.3 = ((f32[2,512]{1,0:T(2,128)S(1)}, f32[2,512]{1,0:T(2,128)S(1)}, f32[2,512,128]{2,1,0:T(8,128)S(1)})) conditional(s32[]{:T(128)} %convert_element_type.114, (f32[2,512]{1,0:T(2,128)S(1)}, f32[2,512]{1,0:T(2,128)S(1)}, f32[2,512,128]{2,1,0:T(8,128)S(1)}) %tuple.53, (s32[]{:T(128)}, s32[]{:T(128)}, s32[]{:T(128)}, ...), branch_computations={%region_4.4_spmd, %region_5.0_spmd} | conditional | flops 274729984 | bytes 9005188 | solution.py:82
  217.5 1.6 fusion.41
  219.6 1.7 convolution_add_fusion
  221.9 4.1 %conditional.3 = ((f32[2,512]{1,0:T(2,128)S(1)}, f32[2,512]{1,0:T(2,128)S(1)}, f32[2,512,128]{2,1,0:T(8,128)S(1)})) conditional(s32[]{:T(128)} %convert_element_type.114, (f32[2,512]{1,0:T(2,128)S(1)}, f32[2,512]{1,0:T(2,128)S(1)}, f32[2,512,128]{2,1,0:T(8,128)S(1)}) %tuple.53, (s32[]{:T(128)}, s32[]{:T(128)}, s32[]{:T(128)}, ...), branch_computations={%region_4.4_spmd, %region_5.0_spmd} | conditional | flops 274729984 | bytes 9005188 | solution.py:82
  222.2 1.6 fusion.41
  224.3 1.7 convolution_add_fusion
  226.6 4.1 %conditional.3 = ((f32[2,512]{1,0:T(2,128)S(1)}, f32[2,512]{1,0:T(2,128)S(1)}, f32[2,512,128]{2,1,0:T(8,128)S(1)})) conditional(s32[]{:T(128)} %convert_element_type.114, (f32[2,512]{1,0:T(2,128)S(1)}, f32[2,512]{1,0:T(2,128)S(1)}, f32[2,512,128]{2,1,0:T(8,128)S(1)}) %tuple.53, (s32[]{:T(128)}, s32[]{:T(128)}, s32[]{:T(128)}, ...), branch_computations={%region_4.4_spmd, %region_5.0_spmd} | conditional | flops 274729984 | bytes 9005188 | solution.py:82
  226.8 1.7 fusion.41
  229.0 1.7 convolution_add_fusion
  231.2 4.0 %conditional.3 = ((f32[2,512]{1,0:T(2,128)S(1)}, f32[2,512]{1,0:T(2,128)S(1)}, f32[2,512,128]{2,1,0:T(8,128)S(1)})) conditional(s32[]{:T(128)} %convert_element_type.114, (f32[2,512]{1,0:T(2,128)S(1)}, f32[2,512]{1,0:T(2,128)S(1)}, f32[2,512,128]{2,1,0:T(8,128)S(1)}) %tuple.53, (s32[]{:T(128)}, s32[]{:T(128)}, s32[]{:T(128)}, ...), branch_computations={%region_4.4_spmd, %region_5.0_spmd} | conditional | flops 274729984 | bytes 9005188 | solution.py:82
  231.5 1.6 fusion.41
  233.6 1.7 convolution_add_fusion
  237.3 1.0 copy.58
  238.3 3.6 all-to-all-start
  241.9 47.3 %reduce-scatter.2.cloned.1.call-done = bf16[128,4,2048]{2,0,1:T(8,128)(2,1)} async-done(((bf16[512,4,2048]{2,0,1:T(8,128)(2,1)}), bf16[128,4,2048]{2,0,1:T(8,128)(2,1)}) %reduce-scatter.2.cloned.1.call-update) | async-done | bytes 2097168 | tf_op jit(solution)/shard_map/reduce_scatter | solution.py:138
  289.2 4.6 %copy.66 = bf16[128,4,2048]{2,1,0:T(4,128)(2,1)} copy(bf16[128,4,2048]{2,0,1:T(8,128)(2,1)} %reduce-scatter.2.cloned.1.call-done) | data formatting | bytes 4194304 | tf_op jit(solution)/shard_map/reduce_scatter | solution.py:138
  293.7 6.2 %all-to-all-start.2 = ((bf16[128,4,2048]{2,1,0:T(4,128)(2,1)}), bf16[128,4,2048]{2,1,0:T(4,128)(2,1)S(1)}, u32[]{:S(2)}, u32[]{:S(2)}) async-start(bf16[128,4,2048]{2,1,0:T(4,128)(2,1)} %copy.66), calls=%async_computation.3 | async-start | bytes 4194304 | tf_op jit(solution)/shard_map/all_to_all | solution.py:146
  300.1 3.7 %fusion.17 = bf16[128,2048]{1,0:T(8,128)(2,1)} fusion(bf16[8,128,128]{2,1,0:T(8,128)(2,1)S(1)} %bitcast.110, bf16[8,128,2048]{2,1,0:T(8,128)(2,1)} %bitcast.109), kind=kOutput, calls=%fused_computation.30 | convolution fusion | flops 537133056 | bytes 4980736 | tf_op jit(solution)/shard_map/hqd,hde->qe/dot_general | solution.py:131
  303.8 40.9 %all-to-all-done.2 = bf16[128,4,2048]{2,1,0:T(4,128)(2,1)S(1)} async-done(((bf16[128,4,2048]{2,1,0:T(4,128)(2,1)}), bf16[128,4,2048]{2,1,0:T(4,128)(2,1)S(1)}, u32[]{:S(2)}, u32[]{:S(2)}) %all-to-all-start.2) | async-done | bytes 2097184 | tf_op jit(solution)/shard_map/all_to_all | solution.py:146
  344.7 2.4 copy.73
  347.1 2.5 reshape.156
  349.6 1.4 gather_fusion.2
  351.0 1.3 reshape.158
  352.3 4.0 %multiply_reduce_fusion = bf16[128,2048]{1,0:T(8,128)(2,1)} fusion(f32[128,2,2048]{2,1,0:T(2,128)S(1)} %reshape.158, f32[128,2]{1,0:T(8,128)S(1)} %copy.68), kind=kLoop, calls=%fused_computation.39 | loop fusion | flops 786432 | bytes 2622464 | tf_op jit(solution)/shard_map/reduce_sum | solution.py:153
  (99 shorter events, 6.6 us)
Async XLA Ops:
  7.2 122.5 %all-gather.8.cloned.1.call-start = ((), (), s32[]{:S(2)}) async-start(), calls=%async_computation.6 | async-start | bytes 10485760 | tf_op jit(solution)/shard_map/all_gather | solution.py:134
  70.8 0.9 copy-start
  70.8 1.1 copy-start.4
  70.9 100.0 %all-gather.4.cloned.1.call-start = ((), (), s32[]{:S(2)}) async-start(), calls=%async_computation.4 | async-start | bytes 1179648 | tf_op jit(solution)/shard_map/all_gather | solution.py:43
  72.7 139.3 %all-gather.6.cloned.1.call-start = ((), (), s32[]{:S(2)}) async-start(), calls=%async_computation.5 | async-start | bytes 1179648 | tf_op jit(solution)/shard_map/all_gather | solution.py:44
  73.5 215.7 %reduce-scatter.2.cloned.1.call-start = ((), (), s32[]{:S(2)}) async-start(), calls=%async_computation.7 | async-start | bytes 10485760 | tf_op jit(solution)/shard_map/reduce_scatter | solution.py:138
  150.5 0.8 copy-start.2
  150.6 3.3 copy-start.1
  150.6 3.6 copy-start.5
  238.3 55.5 %all-to-all-start = ((bf16[2,512,128]{2,0,1:T(2,128)(2,1)}), bf16[2,512,128]{2,0,1:T(2,128)(2,1)S(1)}, u32[]{:S(2)}, u32[]{:S(2)}) async-start(bf16[2,512,128]{2,0,1:T(2,128)(2,1)} %copy.58), calls=%async_computation | async-start | bytes 524288 | tf_op jit(solution)/shard_map/all_to_all | solution.py:128
  293.7 6.2 %copy-start.3 = (f32[128,2]{0,1:T(2,128)S(1)}, f32[128,2]{0,1:T(2,128)}, u32[]{:S(2)}) copy-start(f32[128,2]{0,1:T(2,128)} %param.28) | copy-start | bytes 3076
  293.7 51.0 %all-to-all-start.2 = ((bf16[128,4,2048]{2,1,0:T(4,128)(2,1)}), bf16[128,4,2048]{2,1,0:T(4,128)(2,1)S(1)}, u32[]{:S(2)}, u32[]{:S(2)}) async-start(bf16[128,4,2048]{2,1,0:T(4,128)(2,1)} %copy.66), calls=%async_computation.3 | async-start | bytes 4194304 | tf_op jit(solution)/shard_map/all_to_all | solution.py:146
Sparse Core Ops, SparseCore 0:
  71.0 58.5 all-gather.7
  132.3 38.4 all-gather.3
  173.0 38.9 all-gather.5
  214.4 74.6 reduce-scatter.1
where the time goes:
time: 368 us; the launch traced here: 363 us
  waiting for transfers between devices  202 us (55%)
  blocking collectives  52.3 us (14%)
  matrix products  41.1 us (11%)
  local copies, waits for them, and re-layouts  25 us (7%)
  between operations  14.1 us (4%)
  other arithmetic  12.7 us (3%)
  starting transfers between devices  10.2 us (3%)
  loops' own time  5.11 us (1%)
    all_gather x1, waiting for transfers between devices, on_device(): pieces = lax.all_gather(received, 'tp', axis=0, tiled=True)  55.9 us
    all_to_all x1, blocking collectives, dispatch(): lax.all_to_all(outgoing, 'ep', split_axis=1, concat_axis=0, tiled=True)  52.3 us
    reduce_scatter x1, waiting for transfers between devices, on_device(): lax.psum_scatter(jnp.einsum('ref,edf->red', hidden, w_down, preferred_ele...  47.3 us
    all_gather x1, waiting for transfers between devices, attend(): value_rows = lax.all_gather(values, 'ep', axis=0, tiled=True)  41.2 us
    all_to_all x1, waiting for transfers between devices, on_device(): lax.all_to_all(summed, 'ep', split_axis=0, concat_axis=1, tiled=True)  40.9 us
    all_gather x1, waiting for transfers between devices, attend(): key_matrix_rows = lax.all_gather(normed_k, 'ep', axis=0, tiled=True)  16.4 us
    dot_general x1, matrix products, on_device(): jnp.einsum('ref,edf->red', hidden, w_down, preferred_element_type=jnp.flo...  14 us
    dot_general x5, matrix products, update(): jnp.einsum('hqk,kd->hqd', weights.astype(jnp.bfloat16), block_values, pre...  8.33 us
  transfers between devices with their start and end apart: 6, of which 5 were waited for; matrix products, arithmetic and copies ran while one was open for 15% of the time, Pallas kernels for 0%

commit v1 on v0

v1 whole, which is shorter than its diff:
```python
import functools

import jax
import jax.numpy as jnp
from jax import lax
from jax.experimental import pallas as pl
from jax.experimental.pallas import tpu as pltpu
from jax.sharding import PartitionSpec as P

CAP = 16
EPSILON = 1e-06
NEGATIVE = -1e30
MESH = pl.DeviceIdType.MESH
VMEM_LIMIT = 62 * 1024 * 1024


def rms_scale(inputs, gain):
    inputs = inputs.astype(jnp.float32)
    return inputs * lax.rsqrt(jnp.mean(inputs * inputs, axis=-1, keepdims=True) + EPSILON) * gain


def places(n_tp):
    ep, tp = lax.axis_index("ep"), lax.axis_index("tp")
    core = tp + 1 - 2 * lax.rem(tp, 2)
    across = lax.rem(tp + n_tp // 2, n_tp)
    corner = lax.rem(core + n_tp // 2, n_tp)
    return ep, tp, core, across, corner


def meet(n_ep, n_tp):
    ep, tp = lax.axis_index("ep"), lax.axis_index("tp")
    barrier = pltpu.get_barrier_semaphore()
    for step in range(1, n_ep):
        pl.semaphore_signal(
            barrier, inc=1, device_id=(lax.rem(ep + step, n_ep), tp), device_id_type=MESH
        )
    for step in range(1, n_tp):
        pl.semaphore_signal(
            barrier, inc=1, device_id=(ep, lax.rem(tp + step, n_tp)), device_id_type=MESH
        )
    pl.semaphore_wait(barrier, n_ep + n_tp - 2)


def remote(src, dst, send, recv, ep, tp):
    return pltpu.make_async_remote_copy(
        src_ref=src, dst_ref=dst, send_sem=send, recv_sem=recv, device_id=(ep, tp), device_id_type=MESH
    )


def gather_kernel(
    n_ep,
    n_tp,
    heads,
    outg,
    kv,
    q,
    fq,
    fk,
    pieces,
    att_all,
    kvbuf,
    att,
    high,
    denom,
    accum,
    a_send,
    a_recv,
    x_send,
    x_recv,
    c_send,
    c_recv,
    d_send,
    d_recv,
    k_send,
    k_recv,
    t_send,
    t_recv,
    own_sem,
):
    ep, tp, core, across, corner = places(n_tp)
    rows, head_dim = kv.shape[0], q.shape[1]
    part = rows // n_tp
    scale = head_dim ** (-0.5)
    meet(n_ep, n_tp)

    def kv_copy(source, step):
        return remote(kv, kvbuf.at[source], k_send.at[step], k_recv.at[source], lax.rem(ep + step, n_ep), tp)

    def a_copy(source, step):
        dest = lax.rem(ep + step, n_ep)
        return remote(outg.at[dest], pieces.at[tp, source], a_send.at[step], a_recv.at[source], dest, tp)

    def x_copy(src, owner, source):
        return remote(src, pieces.at[owner, source], x_send.at[source], x_recv.at[source], ep, across)

    def c_copy(src, owner, source):
        return remote(src, pieces.at[owner, source], c_send.at[source], c_recv.at[source], ep, core)

    def d_copy(src, owner, source):
        return remote(src, pieces.at[owner, source], d_send.at[source], d_recv.at[source], ep, core)

    def start_kv(step, carry):
        @pl.when(ep + step < n_ep)
        def _():
            kv_copy(ep, step).start()

        return carry

    lax.fori_loop(1, n_ep, start_kv, 0)
    own = pltpu.make_async_copy(outg.at[ep], pieces.at[tp, ep], own_sem)
    own.start()
    x_copy(outg.at[ep], tp, ep).start()
    c_copy(outg.at[ep], tp, ep).start()

    def start_a(step, carry):
        a_copy(ep, step).start()
        return carry

    lax.fori_loop(1, n_ep, start_a, 0)

    tile = rows // 2

    def block(source, keys_ref, diagonal):
        keys = keys_ref[:, :head_dim]
        vals = keys_ref[:, head_dim:]
        for head in range(heads):
            key_gate = fk[source, head : head + 1, :]
            for half in range(2):
                span = pl.ds(head * rows + half * tile, tile)
                scores = lax.dot_general(
                    q[span, :], keys, (((1,), (1,)), ((), ())), preferred_element_type=jnp.float32
                )
                scores = scores * scale + fq[span, :] - key_gate
                if diagonal:
                    qpos = half * tile + lax.broadcasted_iota(jnp.int32, scores.shape, 0)
                    kpos = lax.broadcasted_iota(jnp.int32, scores.shape, 1)
                    scores = jnp.where(kpos <= qpos, scores, NEGATIVE)
                top = jnp.max(scores, axis=1, keepdims=True)
                if diagonal:
                    newest = top
                else:
                    before = high[span, :]
                    newest = jnp.maximum(before, top)
                weights = jnp.exp(scores - newest)
                total = jnp.sum(weights, axis=1, keepdims=True)
                product = jnp.dot(
                    weights.astype(jnp.bfloat16), vals, preferred_element_type=jnp.float32
                )
                if not diagonal:
                    factor = jnp.exp(before - newest)
                    total = denom[span, :] * factor + total
                    product = accum[span, :] * factor + product
                high[span, :] = newest
                denom[span, :] = total
                accum[span, :] = product

    block(ep, kv, True)

    def relay(source):
        x_copy(outg.at[ep], across, source).wait_recv()
        d_copy(pieces.at[across, source], across, source).start()

    def onward(step, carry):
        source = lax.rem(ep - step + n_ep, n_ep)
        a_copy(source, step).wait_recv()
        x_copy(pieces.at[tp, source], tp, source).start()
        c_copy(pieces.at[tp, source], tp, source).start()

        @pl.when(ep - step >= 0)
        def _():
            kv_copy(source, step).wait_recv()
            block(source, kvbuf.at[source], False)

        relay(lax.rem(source + 1, n_ep))
        return carry

    lax.fori_loop(1, n_ep, onward, 0)

    for head in range(heads):
        span = pl.ds(head * rows, rows)
        result = (accum[span, :] / denom[span, :]).astype(jnp.bfloat16)
        for owner in range(n_tp):
            att[owner, head] = result[owner * part : (owner + 1) * part]
    relay(lax.rem(ep + 1, n_ep))

    def t_copy(source, step):
        dest = lax.rem(tp + step, n_tp)
        return remote(att.at[dest], att_all.at[source], t_send.at[step], t_recv.at[source], ep, dest)

    for step in range(1, n_tp):
        t_copy(tp, step).start()
    att_all[tp] = att[tp]

    def finish(source, carry):
        c_copy(outg.at[ep], core, source).wait()
        d_copy(outg.at[ep], corner, source).wait()
        x_copy(outg.at[ep], tp, source).wait_send()
        return carry

    lax.fori_loop(0, n_ep, finish, 0)

    def sent(step, carry):
        a_copy(ep, step).wait_send()

        @pl.when(ep + step < n_ep)
        def _():
            kv_copy(ep, step).wait_send()

        return carry

    lax.fori_loop(1, n_ep, sent, 0)
    for step in range(1, n_tp):
        t_copy(lax.rem(tp - step + n_tp, n_tp), step).wait()
    own.wait()


def expert_kernel(x, gate_w, up_w, down_w, out):
    blocks, _, cap, width = x.shape
    chunk = min(blocks, 512 // cap)

    def some(number, carry):
        span = pl.ds(number * chunk, chunk)
        rows = x[span, 0].reshape(chunk * cap, width)
        gate = jnp.dot(rows, gate_w[0], preferred_element_type=jnp.float32)
        upward = jnp.dot(rows, up_w[0], preferred_element_type=jnp.float32)
        hidden = (gate / (1.0 + jnp.exp(-gate)) * upward).astype(jnp.bfloat16)
        result = lax.dot_general(
            hidden, down_w[0], (((1,), (1,)), ((), ())), preferred_element_type=jnp.float32
        )
        out[span, 0] = result.astype(jnp.bfloat16).reshape(chunk, cap, width)
        return carry

    lax.fori_loop(0, blocks // chunk, some, 0)


def return_kernel(
    n_ep,
    n_tp,
    part_ref,
    att_all,
    mixer,
    slots,
    route_weights,
    mixed,
    routed,
    near_own,
    near_far,
    sum_x,
    got_x,
    sum_r,
    back,
    n_send,
    n_recv,
    f_send,
    f_recv,
    x_send,
    x_recv,
    r_send,
    r_recv,
):
    ep, tp, core, across, corner = places(n_tp)
    meet(n_ep, n_tp)

    def far_copy(dest):
        return remote(part_ref.at[corner, dest], near_far.at[dest], f_send.at[dest], f_recv.at[dest], ep, core)

    def own_copy(dest):
        return remote(part_ref.at[core, dest], near_own.at[dest], n_send.at[dest], n_recv.at[dest], ep, core)

    def x_copy(dest):
        return remote(sum_x.at[dest], got_x.at[dest], x_send.at[dest], x_recv.at[dest], ep, across)

    def r_copy(source, dest):
        return remote(sum_r.at[dest], back.at[source], r_send.at[dest], r_recv.at[source], dest, tp)

    def order(step):
        return lax.rem(ep + step, n_ep)

    def start_far(step, carry):
        far_copy(order(step)).start()
        return carry

    def start_own(step, carry):
        own_copy(order(step)).start()
        return carry

    lax.fori_loop(1, n_ep + 1, start_far, 0)
    lax.fori_loop(1, n_ep + 1, start_own, 0)

    def first(step, carry):
        dest = order(step)
        far_copy(dest).wait_recv()
        sum_x[dest] = (
            part_ref[across, dest].astype(jnp.float32) + near_far[dest].astype(jnp.float32)
        ).astype(jnp.bfloat16)
        x_copy(dest).start()
        return carry

    lax.fori_loop(1, n_ep + 1, first, 0)

    sources, heads, part, head_dim = att_all.shape
    total = None
    for source in range(sources):
        for head in range(heads):
            number = source * heads + head
            term = jnp.dot(
                att_all[source, head],
                mixer[number * head_dim : (number + 1) * head_dim, :],
                preferred_element_type=jnp.float32,
            )
            total = term if total is None else total + term
    mixed[...] = total.astype(jnp.bfloat16)

    def second(dest):
        own_copy(dest).wait_recv()
        x_copy(dest).wait_recv()
        return (
            part_ref[tp, dest].astype(jnp.float32)
            + near_own[dest].astype(jnp.float32)
            + got_x[dest].astype(jnp.float32)
        ).astype(jnp.bfloat16)

    def send_back(step, carry):
        dest = order(step)
        sum_r[dest] = second(dest)
        r_copy(ep, dest).start()
        return carry

    lax.fori_loop(1, n_ep, send_back, 0)
    back[ep] = second(ep)

    def arrived(step, carry):
        source = lax.rem(ep - step + n_ep, n_ep)
        r_copy(source, order(step)).wait()
        return carry

    lax.fori_loop(1, n_ep, arrived, 0)

    def sent(dest, carry):
        far_copy(dest).wait_send()
        own_copy(dest).wait_send()
        x_copy(dest).wait_send()
        return carry

    lax.fori_loop(0, n_ep, sent, 0)

    _, per, width = back.shape
    rows = back[...].reshape(n_ep * per, width)
    summed = None
    for choice in range(slots.shape[1]):
        lanes = lax.broadcasted_iota(jnp.int32, (slots.shape[0], n_ep * per), 1)
        pick = jnp.where(lanes == slots[:, choice : choice + 1], 1.0, 0.0).astype(jnp.bfloat16)
        found = jnp.dot(pick, rows, preferred_element_type=jnp.float32)
        term = found * route_weights[:, choice : choice + 1]
        summed = term if summed is None else summed + term
    routed[...] = summed.astype(jnp.bfloat16)


def on_device(
    n_ep,
    n_tp,
    queries,
    keys,
    values,
    forget_cache,
    query_gain,
    key_gain,
    mixer_out,
    expert_input,
    norm_gain,
    routes,
    route_weights,
    w_gate,
    w_up,
    w_down,
):
    rows, head_dim = keys.shape
    heads = forget_cache.shape[0]
    ep = lax.axis_index("ep")
    local, width, ff = w_gate.shape
    experts = local * n_ep
    tokens = expert_input.shape[0]
    per = local * CAP
    part = rows // n_tp
    vmem = pl.BlockSpec(memory_space=pltpu.VMEM)
    anywhere = pl.BlockSpec(memory_space=pl.ANY)
    dma = pltpu.SemaphoreType.DMA

    normed_q = rms_scale(queries.reshape(rows, heads, head_dim), query_gain).astype(jnp.bfloat16)
    q = normed_q.transpose(1, 0, 2).reshape(heads * rows, head_dim)
    kv = jnp.concatenate([rms_scale(keys, key_gain).astype(jnp.bfloat16), values], axis=1)
    fq = lax.dynamic_slice_in_dim(forget_cache, ep * rows, rows, 1).reshape(heads * rows, 1)
    fk = forget_cache.reshape(heads, n_ep, rows).transpose(1, 0, 2)

    normed = rms_scale(expert_input, norm_gain).astype(jnp.bfloat16)
    names = jnp.arange(experts, dtype=jnp.int32)
    named = [(routes[:, k : k + 1] == names[None, :]) for k in range(routes.shape[1])]
    anyone = functools.reduce(jnp.logical_or, named).astype(jnp.bfloat16)
    at = jnp.arange(tokens, dtype=jnp.int32)
    earlier = (at[None, :] < at[:, None]).astype(jnp.bfloat16)
    prior = jnp.dot(earlier, anyone, preferred_element_type=jnp.float32)
    ranks = [jnp.sum(jnp.where(mine, prior, 0.0), axis=1).astype(jnp.int32) for mine in named]
    slots = jnp.stack([routes[:, k] * CAP + rank for k, rank in enumerate(ranks)], axis=1)
    line = jnp.arange(experts * CAP, dtype=jnp.int32)[:, None]
    place = functools.reduce(
        jnp.logical_or, [line == slots[:, k][None, :] for k in range(slots.shape[1])]
    ).astype(jnp.bfloat16)
    outg = jnp.dot(place, normed, preferred_element_type=jnp.float32).astype(jnp.bfloat16)
    outg = outg.reshape(n_ep, per, width)

    pieces, att_all = pl.pallas_call(
        functools.partial(gather_kernel, n_ep, n_tp, heads),
        out_shape=(
            jax.ShapeDtypeStruct((n_tp, n_ep, per, width), jnp.bfloat16),
            jax.ShapeDtypeStruct((n_tp, heads, part, head_dim), jnp.bfloat16),
        ),
        in_specs=[vmem] * 5,
        out_specs=(anywhere, vmem),
        scratch_shapes=[
            pltpu.VMEM((n_ep, rows, 2 * head_dim), jnp.bfloat16),
            pltpu.VMEM((n_tp, heads, part, head_dim), jnp.bfloat16),
            pltpu.VMEM((heads * rows, 1), jnp.float32),
            pltpu.VMEM((heads * rows, 1), jnp.float32),
            pltpu.VMEM((heads * rows, head_dim), jnp.float32),
        ]
        + [dma((n_ep,))] * 10
        + [dma((n_tp,))] * 2
        + [dma],
        compiler_params=pltpu.CompilerParams(
            collective_id=0, has_side_effects=True, vmem_limit_bytes=VMEM_LIMIT
        ),
        name="gather",
    )(outg, kv, q, fq, fk)

    blocks = n_tp * n_ep
    row_spec = pl.BlockSpec((blocks, 1, CAP, width), lambda e: (0, e, 0, 0))
    weight_spec = pl.BlockSpec((1, width, ff), lambda e: (e, 0, 0))
    partial_sums = pl.pallas_call(
        expert_kernel,
        out_shape=jax.ShapeDtypeStruct((blocks, local, CAP, width), jnp.bfloat16),
        grid=(local,),
        in_specs=[row_spec, weight_spec, weight_spec, weight_spec],
        out_specs=row_spec,
        compiler_params=pltpu.CompilerParams(vmem_limit_bytes=VMEM_LIMIT),
        name="experts",
    )(pieces.reshape(blocks, local, CAP, width), w_gate, w_up, w_down)
    partial_sums = partial_sums.reshape(n_tp, n_ep, per, width)

    buffer = pltpu.VMEM((n_ep, per, width), jnp.bfloat16)
    return pl.pallas_call(
        functools.partial(return_kernel, n_ep, n_tp),
        out_shape=(
            jax.ShapeDtypeStruct((part, width), jnp.bfloat16),
            jax.ShapeDtypeStruct((tokens, width), jnp.bfloat16),
        ),
        in_specs=[vmem] * 5,
        out_specs=(vmem, vmem),
        scratch_shapes=[buffer] * 6 + [dma((n_ep,))] * 8,
        compiler_params=pltpu.CompilerParams(
            collective_id=1, has_side_effects=True, vmem_limit_bytes=VMEM_LIMIT
        ),
        name="give_back",
    )(partial_sums, att_all, mixer_out, slots, route_weights)


def solution(mesh):
    n_ep, n_tp = mesh.shape["ep"], mesh.shape["tp"]
    in_specs = (
        P("ep", "tp"),
        P("ep", "tp"),
        P("ep", "tp"),
        P("tp", None),
        P(),
        P(),
        P(),
        P(("ep", "tp"), None),
        P(),
        P(("ep", "tp"), None),
        P(("ep", "tp"), None),
        P("ep", None, "tp"),
        P("ep", None, "tp"),
        P("ep", None, "tp"),
    )
    out_specs = (P(("ep", "tp"), None), P(("ep", "tp"), None))
    return jax.shard_map(
        functools.partial(on_device, n_ep, n_tp),
        mesh=mesh,
        in_specs=in_specs,
        out_specs=out_specs,
        check_vma=False,
    )
```

time: 368 us -> 229 us (0.62)
  Pallas kernels: 0 us -> 208 us
  waiting for transfers between devices: 202 us -> 0 us
  blocking collectives: 52.3 us -> 0 us
  matrix products: 41.1 us -> 3.38 us
  local copies, waits for them, and re-layouts: 25 us -> 9.72 us
  between operations: 14.1 us -> 0.78 us
  starting transfers between devices: 10.2 us -> 0 us
  other arithmetic: 12.7 us -> 4.42 us
  loops' own time: 5.11 us -> 0 us
    pallas_call x0 -> x3, Pallas kernels: none -> 208 us  [the longest x1 126 us: on_device(): pl.pallas_call(functools.partial(gather_kernel, n_ep, n_tp, heads), out_s...]
    all_gather x3 -> x0, waiting for transfers between devices: 114 us -> none  [the longest x1 55.9 us: on_device(): pieces = lax.all_gather(received, 'tp', axis=0, tiled=True)]
    all_to_all x1 -> x0, blocking collectives: 52.3 us -> none  [dispatch(): lax.all_to_all(outgoing, 'ep', split_axis=1, concat_axis=0, tiled=True)]
    reduce_scatter x1 -> x0, waiting for transfers between devices: 47.3 us -> none  [on_device(): lax.psum_scatter(jnp.einsum('ref,edf->red', hidden, w_down, preferred_ele...]
    all_to_all x2 -> x0, waiting for transfers between devices: 40.9 us -> none  [the longest x1 40.9 us: on_device(): lax.all_to_all(summed, 'ep', split_axis=0, concat_axis=1, tiled=True)]
    dot_general x13 -> x2, matrix products: 41.1 us -> 3.38 us  [the longest x1 3.23 us: on_device(): jnp.dot(place, normed, preferred_element_type=jnp.float32)]
    all_to_all x2 -> x0, starting transfers between devices: 9.81 us -> none  [the longest x1 6.18 us: on_device(): lax.all_to_all(summed, 'ep', split_axis=0, concat_axis=1, tiled=True)]
    reduce_sum x7 -> x0, other arithmetic: 6.28 us -> none  [the longest x1 4.04 us: on_device(): jnp.sum(picked * route_weights[:, :, None], axis=1).astype(jnp.bfloat16)]
  transfers between devices with their start and end apart: 6 -> 0, of which waited for: 5 -> 0; matrix products, arithmetic and copies ran while one was open for 15% -> 0% of each run, Pallas kernels for 0% -> 0%
where the time goes in v1:
time: 229 us; the launch traced here: 226 us
  Pallas kernels  208 us (91%)
  local copies, waits for them, and re-layouts  9.72 us (4%)
  other arithmetic  4.42 us (2%)
  matrix products  3.38 us (1%)
    pallas_call x1, Pallas kernels, on_device(): pl.pallas_call(functools.partial(gather_kernel, n_ep, n_tp, heads), out_s...  126 us
    pallas_call x1, Pallas kernels, on_device(): pl.pallas_call(functools.partial(return_kernel, n_ep, n_tp), out_shape=(j...  69 us
    pallas_call x1, Pallas kernels, on_device(): pl.pallas_call(expert_kernel, out_shape=jax.ShapeDtypeStruct((blocks, loc...  13.2 us
    unnamed x18, local copies, waits for them, and re-layouts  6.26 us

profile of v1, /device:TPU:16, one launch (start us, length us, event | category | flops | bytes accessed | tf_op | source)
XLA Modules:
  0.0 226.1 jit_solution(2566385394705595350)
XLA Ops:
  0.6 0.0 copy-start.4
  0.6 0.0 copy-start
  0.7 0.0 copy-start.5
  0.7 0.0 copy-start.1
  0.7 0.8 slice_bitcast_fusion.1
  1.4 0.2 select_reduce_fusion.1
  1.6 0.8 convert_add_fusion.1
  2.4 1.2 fusion
  3.6 3.2 %convolution_convert_fusion = bf16[512,2048]{1,0:T(8,128)(2,1)} fusion(bf16[128,2048]{1,0:T(8,128)(2,1)} %param.21, f32[2048]{0:T(1024)} %param.22, f32[128]{0:T(128)S(1)} %add_rsqrt_fusion.2, s32[128]{0:T(128)S(1)} %get-tuple-element.11, s32[128]{0:T(128)S(1)} %get-tuple-element.10), kind=kOutput, calls=%fused_computation | convolution fusion | flops 270729216 | bytes 2631168 | tf_op jit(solution)/shard_map/dot_general | solution.py:408
  6.8 0.7 dynamic-slice_bitcast_fusion
  7.5 1.0 copy.40
  8.6 1.2 reshape.92
  9.8 0.6 multiply_reduce_fusion
  10.4 0.0 copy-done.4
  10.4 0.7 fusion.9
  11.2 0.8 copy.35
  11.9 0.0 copy-done
  11.9 0.1 fusion.6
  12.1 0.0 copy-done.5
  12.1 0.1 fusion.8
  12.2 0.0 copy-done.1
  12.3 0.7 pad_maximum_fusion.kv
  13.0 125.6 %gather.1 = (bf16[4,8,64,2048]{3,2,1,0:T(8,128)(2,1)}, bf16[4,2,128,128]{3,2,1,0:T(8,128)(2,1)}) custom-call(bf16[8,64,2048]{2,1,0:T(8,128)(2,1)} %bitcast.28, bf16[512,256]{1,0:T(8,128)(2,1)} %pad_maximum_fusion.kv, bf16[1024,128]{1,0:T(8,128)(2,1)} %bitcast.30, f32[1024,1]{1,0:T(8,128)} %bitcast.29, f32[8,2,512]{2,1,0:T(2,128)} %bitcast.31), custom_call_target="tpu_custom_call" | custom-call | tf_op jit(solution)/shard_map/gather/pallas_call | solution.py:411
  138.6 0.0 copy-start.2
  138.6 0.0 copy-start.3
  138.6 13.2 %experts.1 = bf16[32,4,16,2048]{3,2,1,0:T(8,128)(2,1)} custom-call(bf16[32,4,16,2048]{3,2,1,0:T(8,128)(2,1)} %bitcast.27, bf16[4,2048,256]{2,1,0:T(8,128)(2,1)} %gate_w.1, bf16[4,2048,256]{2,1,0:T(8,128)(2,1)} %up_w.1, bf16[4,2048,256]{2,1,0:T(8,128)(2,1)} %down_w.1), custom_call_target="tpu_custom_call" | custom-call | tf_op jit(solution)/shard_map/experts/pallas_call | solution.py:438
  151.9 0.0 copy-done.2
  151.9 0.7 copy.37.slots
  152.6 0.0 copy-done.3
  152.6 0.7 copy.38.route_weights
  153.4 69.0 %give_back.1 = (bf16[128,2048]{1,0:T(8,128)(2,1)}, bf16[128,2048]{1,0:T(8,128)(2,1)}) custom-call(bf16[4,8,64,2048]{3,2,1,0:T(8,128)(2,1)} %bitcast.26, bf16[4,2,128,128]{3,2,1,0:T(8,128)(2,1)} %get-tuple-element.5.att_all, bf16[1024,2048]{1,0:T(8,128)(2,1)} %mixer.1, s32[128,2]{1,0:T(8,128)} %copy.37.slots, f32[128,2]{1,0:T(8,128)} %copy.38.route_weights), custom_call_target="tpu_custom_call" | custom-call | tf_op jit(solution)/shard_map/give_back/pallas_call | solution.py:450
  222.4 1.9 copy.44
  224.2 1.9 copy.45
  (6 shorter events, 0.1 us)
Async XLA Ops:
  0.6 9.8 %copy-start.4 = (f32[128]{0:T(128)S(1)}, f32[128]{0:T(128)}, u32[]{:S(2)}) copy-start(f32[128]{0:T(128)} %param.18) | copy-start | bytes 1540
  0.6 11.3 %copy-start = (bf16[512,128]{1,0:T(8,128)(2,1)S(1)}, bf16[512,128]{1,0:T(8,128)(2,1)}, u32[]{:S(2)}) copy-start(bf16[512,128]{1,0:T(8,128)(2,1)} %param.15) | copy-start | bytes 393220
  0.7 11.4 %copy-start.5 = (f32[128]{0:T(128)S(1)}, f32[128]{0:T(128)}, u32[]{:S(2)}) copy-start(f32[128]{0:T(128)} %param.19) | copy-start | bytes 1540
  0.7 11.6 %copy-start.1 = (bf16[512,128]{1,0:T(8,128)(2,1)S(1)}, bf16[512,128]{1,0:T(8,128)(2,1)}, u32[]{:S(2)}) copy-start(bf16[512,128]{1,0:T(8,128)(2,1)} %param.16) | copy-start | bytes 393220
  138.6 13.3 %copy-start.2 = (s32[128,2]{0,1:T(2,128)S(1)}, s32[128,2]{0,1:T(2,128)}, u32[]{:S(2)}) copy-start(s32[128,2]{0,1:T(2,128)} %param.23) | copy-start | bytes 3076
  138.6 14.0 %copy-start.3 = (f32[128,2]{0,1:T(2,128)S(1)}, f32[128,2]{0,1:T(2,128)}, u32[]{:S(2)}) copy-start(f32[128,2]{0,1:T(2,128)} %param.24) | copy-start | bytes 3076

commit v2 on v1

--- a/solution.py
+++ b/solution.py
@@ -25,6 +25,14 @@
     across = lax.rem(tp + n_tp // 2, n_tp)
     corner = lax.rem(core + n_tp // 2, n_tp)
     return ep, tp, core, across, corner
+
+
+def paired(place, step, count):
+    result, bit = 0, 1
+    while bit < count:
+        result = result + bit * lax.rem(lax.div(place, bit) + lax.div(step, bit), 2)
+        bit *= 2
+    return result
 
 
 def meet(n_ep, n_tp):
@@ -71,6 +79,7 @@
     c_recv,
     d_send,
     d_recv,
+    u_send,
     k_send,
     k_recv,
     t_send,
@@ -83,12 +92,26 @@
     scale = head_dim ** (-0.5)
     meet(n_ep, n_tp)
 
-    def kv_copy(source, step):
-        return remote(kv, kvbuf.at[source], k_send.at[step], k_recv.at[source], lax.rem(ep + step, n_ep), tp)
-
-    def a_copy(source, step):
-        dest = lax.rem(ep + step, n_ep)
-        return remote(outg.at[dest], pieces.at[tp, source], a_send.at[step], a_recv.at[source], dest, tp)
+    level, side = lax.div(ep, 2), lax.rem(ep, 2)
+    levels = n_ep // 2
+    beside = ep + 1 - 2 * side
+
+    def up_copy(src, source):
+        above = lax.rem(ep + 2, n_ep)
+        return remote(src, kvbuf.at[source], u_send.at[source], k_recv.at[source], above, tp)
+
+    def side_copy(src, source):
+        return remote(src, kvbuf.at[source], k_send.at[source], k_recv.at[source], beside, tp)
+
+    def a_copy(step):
+        other = paired(ep, step, n_ep)
+        return remote(outg.at[other], pieces.at[tp, ep], a_send.at[other], a_recv.at[ep], other, tp)
+
+    def a_wait(step):
+        other = paired(ep, step, n_ep)
+        remote(
+            outg.at[other], pieces.at[tp, other], a_send.at[other], a_recv.at[other], other, tp
+        ).wait_recv()
 
     def x_copy(src, owner, source):
         return remote(src, pieces.at[owner, source], x_send.at[source], x_recv.at[source], ep, across)
@@ -99,24 +122,25 @@
     def d_copy(src, owner, source):
         return remote(src, pieces.at[owner, source], d_send.at[source], d_recv.at[source], ep, core)
 
-    def start_kv(step, carry):
-        @pl.when(ep + step < n_ep)
-        def _():
-            kv_copy(ep, step).start()
-
-        return carry
-
-    lax.fori_loop(1, n_ep, start_kv, 0)
+    @pl.when(level + 1 < levels)
+    def _():
+        up_copy(kv, ep).start()
+
+    @pl.when(side == 0)
+    def _():
+        side_copy(kv, ep).start()
+
     own = pltpu.make_async_copy(outg.at[ep], pieces.at[tp, ep], own_sem)
     own.start()
     x_copy(outg.at[ep], tp, ep).start()
     c_copy(outg.at[ep], tp, ep).start()
 
     def start_a(step, carry):
-        a_copy(ep, step).start()
-        return carry
-
-    lax.fori_loop(1, n_ep, start_a, 0)
+        a_copy(step).start()
+        return carry
+
+    near = min(4, n_ep)
+    lax.fori_loop(1, near, start_a, 0)
 
     tile = rows // 2
 
@@ -154,24 +178,54 @@
                 denom[span, :] = total
                 accum[span, :] = product
 
-    block(ep, kv, True)
+    def spread(source):
+        side_copy(kvbuf.at[source], source).start()
+
+        @pl.when(level + 1 < levels)
+        def _():
+            up_copy(kvbuf.at[source], source).start()
 
     def relay(source):
         x_copy(outg.at[ep], across, source).wait_recv()
         d_copy(pieces.at[across, source], across, source).start()
 
+    @pl.when(level > 0)
+    def _():
+        side_copy(kv, ep - 2).wait_recv()
+        spread(ep - 2)
+
+    lax.fori_loop(near, n_ep, start_a, 0)
+
+    block(ep, kv, True)
+
+    @pl.when(side == 1)
+    def _():
+        side_copy(kv, ep - 1).wait_recv()
+        block(ep - 1, kvbuf.at[ep - 1], False)
+
     def onward(step, carry):
-        source = lax.rem(ep - step + n_ep, n_ep)
-        a_copy(source, step).wait_recv()
+        source = paired(ep, step, n_ep)
+        a_wait(step)
         x_copy(pieces.at[tp, source], tp, source).start()
         c_copy(pieces.at[tp, source], tp, source).start()
 
-        @pl.when(ep - step >= 0)
+        below = level - lax.div(step + 1, 2)
+        turned = lax.rem(step + 1, 2)
+        lower = 2 * below + lax.rem(side + turned, 2)
+
+        @pl.when(below >= 0)
         def _():
-            kv_copy(source, step).wait_recv()
-            block(source, kvbuf.at[source], False)
-
-        relay(lax.rem(source + 1, n_ep))
+            @pl.when(step > 1)
+            def _():
+                side_copy(kv, lower).wait_recv()
+
+                @pl.when(turned == 0)
+                def _():
+                    spread(lower)
+
+            block(lower, kvbuf.at[lower], False)
+
+        relay(paired(ep, step - 1, n_ep))
         return carry
 
     lax.fori_loop(1, n_ep, onward, 0)
@@ -181,7 +235,7 @@
         result = (accum[span, :] / denom[span, :]).astype(jnp.bfloat16)
         for owner in range(n_tp):
             att[owner, head] = result[owner * part : (owner + 1) * part]
-    relay(lax.rem(ep + 1, n_ep))
+    relay(paired(ep, n_ep - 1, n_ep))
 
     def t_copy(source, step):
         dest = lax.rem(tp + step, n_tp)
@@ -200,15 +254,30 @@
     lax.fori_loop(0, n_ep, finish, 0)
 
     def sent(step, carry):
-        a_copy(ep, step).wait_send()
-
-        @pl.when(ep + step < n_ep)
+        a_copy(step).wait_send()
+        return carry
+
+    lax.fori_loop(1, n_ep, sent, 0)
+
+    @pl.when(level + 1 < levels)
+    def _():
+        up_copy(kv, ep).wait_send()
+
+    @pl.when(side == 0)
+    def _():
+        side_copy(kv, ep).wait_send()
+
+    def spread_sent(k, carry):
+        source = ep - 2 * k
+        side_copy(kv, source).wait_send()
+
+        @pl.when(level + 1 < levels)
         def _():
-            kv_copy(ep, step).wait_send()
-
-        return carry
-
-    lax.fori_loop(1, n_ep, sent, 0)
+            up_copy(kv, source).wait_send()
+
+        return carry
+
+    lax.fori_loop(1, level + 1, spread_sent, 0)
     for step in range(1, n_tp):
         t_copy(lax.rem(tp - step + n_tp, n_tp), step).wait()
     own.wait()
@@ -239,8 +308,7 @@
     part_ref,
     att_all,
     mixer,
-    slots,
-    route_weights,
+    slots_weights,
     mixed,
     routed,
     near_own,
@@ -274,7 +342,7 @@
         return remote(sum_r.at[dest], back.at[source], r_send.at[dest], r_recv.at[source], dest, tp)
 
     def order(step):
-        return lax.rem(ep + step, n_ep)
+        return paired(ep, n_ep - step, n_ep)
 
     def start_far(step, carry):
         far_copy(order(step)).start()
@@ -330,8 +398,8 @@
     back[ep] = second(ep)
 
     def arrived(step, carry):
-        source = lax.rem(ep - step + n_ep, n_ep)
-        r_copy(source, order(step)).wait()
+        other = order(step)
+        r_copy(other, other).wait()
         return carry
 
     lax.fori_loop(1, n_ep, arrived, 0)
@@ -347,11 +415,12 @@
     _, per, width = back.shape
     rows = back[...].reshape(n_ep * per, width)
     summed = None
-    for choice in range(slots.shape[1]):
-        lanes = lax.broadcasted_iota(jnp.int32, (slots.shape[0], n_ep * per), 1)
-        pick = jnp.where(lanes == slots[:, choice : choice + 1], 1.0, 0.0).astype(jnp.bfloat16)
+    top = slots_weights.shape[1] // 2
+    for choice in range(top):
+        lanes = lax.broadcasted_iota(jnp.int32, (mixed.shape[0], n_ep * per), 1)
+        pick = jnp.where(lanes.astype(jnp.float32) == slots_weights[:, choice : choice + 1], 1.0, 0.0).astype(jnp.bfloat16)
         found = jnp.dot(pick, rows, preferred_element_type=jnp.float32)
-        term = found * route_weights[:, choice : choice + 1]
+        term = found * slots_weights[:, top + choice : top + choice + 1]
         summed = term if summed is None else summed + term
     routed[...] = summed.astype(jnp.bfloat16)
 
@@ -401,6 +470,7 @@
     prior = jnp.dot(earlier, anyone, preferred_element_type=jnp.float32)
     ranks = [jnp.sum(jnp.where(mine, prior, 0.0), axis=1).astype(jnp.int32) for mine in named]
     slots = jnp.stack([routes[:, k] * CAP + rank for k, rank in enumerate(ranks)], axis=1)
+    slots_weights = jnp.concatenate([slots.astype(jnp.float32), route_weights], axis=1)
     line = jnp.arange(experts * CAP, dtype=jnp.int32)[:, None]
     place = functools.reduce(
         jnp.logical_or, [line == slots[:, k][None, :] for k in range(slots.shape[1])]
@@ -423,7 +493,7 @@
             pltpu.VMEM((heads * rows, 1), jnp.float32),
             pltpu.VMEM((heads * rows, head_dim), jnp.float32),
         ]
-        + [dma((n_ep,))] * 10
+        + [dma((n_ep,))] * 11
         + [dma((n_tp,))] * 2
         + [dma],
         compiler_params=pltpu.CompilerParams(
@@ -453,14 +523,14 @@
             jax.ShapeDtypeStruct((part, width), jnp.bfloat16),
             jax.ShapeDtypeStruct((tokens, width), jnp.bfloat16),
         ),
-        in_specs=[vmem] * 5,
+        in_specs=[vmem] * 4,
         out_specs=(vmem, vmem),
         scratch_shapes=[buffer] * 6 + [dma((n_ep,))] * 8,
         compiler_params=pltpu.CompilerParams(
             collective_id=1, has_side_effects=True, vmem_limit_bytes=VMEM_LIMIT
         ),
         name="give_back",
-    )(partial_sums, att_all, mixer_out, slots, route_weights)
+    )(partial_sums, att_all, mixer_out, slots_weights)
 
 
 def solution(mesh):

time: 229 us -> 181 us (0.79)
  the two profiles are of different devices: /device:TPU:16 before, /device:TPU:0 now
where the time goes in v2:
time: 181 us; the launch traced here: 180 us
  Pallas kernels  163 us (90%)
  local copies, waits for them, and re-layouts  8.98 us (5%)
  other arithmetic  4.43 us (2%)
  matrix products  3.38 us (2%)
    pallas_call x1, Pallas kernels, on_device(): pl.pallas_call(functools.partial(return_kernel, n_ep, n_tp), out_shape=(j...  75.6 us
    pallas_call x1, Pallas kernels, on_device(): pl.pallas_call(functools.partial(gather_kernel, n_ep, n_tp, heads), out_s...  74 us
    pallas_call x1, Pallas kernels, on_device(): pl.pallas_call(expert_kernel, out_shape=jax.ShapeDtypeStruct((blocks, loc...  13.2 us
    unnamed x17, local copies, waits for them, and re-layouts  5.51 us

profile of v2, /device:TPU:0, one launch (start us, length us, event | category | flops | bytes accessed | tf_op | source)
XLA Modules:
  0.0 180.4 jit_solution(15694749583145811486)
XLA Ops:
  0.6 0.0 copy-start.4
  0.6 0.0 copy-start
  0.7 0.0 copy-start.5
  0.7 0.0 copy-start.1
  0.7 0.8 slice_bitcast_fusion.1
  1.4 0.2 select_reduce_fusion.1
  1.6 0.8 convert_add_fusion.1
  2.4 1.2 fusion
  3.6 3.2 %convolution_convert_fusion = bf16[512,2048]{1,0:T(8,128)(2,1)} fusion(bf16[128,2048]{1,0:T(8,128)(2,1)} %param.21, f32[2048]{0:T(1024)} %param.22, f32[128]{0:T(128)S(1)} %add_rsqrt_fusion.2, s32[128]{0:T(128)S(1)} %get-tuple-element.11, s32[128]{0:T(128)S(1)} %get-tuple-element.10), kind=kOutput, calls=%fused_computation | convolution fusion | flops 270729216 | bytes 2631168 | tf_op jit(solution)/shard_map/dot_general | solution.py:478
  6.8 0.7 dynamic-slice_bitcast_fusion
  7.5 1.0 copy.38
  8.6 1.2 reshape.92
  9.8 0.6 multiply_reduce_fusion
  10.4 0.0 copy-done.4
  10.4 0.7 fusion.9
  11.2 0.8 copy.34
  11.9 0.0 copy-done
  11.9 0.1 fusion.6
  12.1 0.0 copy-done.5
  12.1 0.1 fusion.8
  12.2 0.0 copy-done.1
  12.3 0.7 pad_maximum_fusion.kv
  13.0 74.0 %gather.1 = (bf16[4,8,64,2048]{3,2,1,0:T(8,128)(2,1)}, bf16[4,2,128,128]{3,2,1,0:T(8,128)(2,1)}) custom-call(bf16[8,64,2048]{2,1,0:T(8,128)(2,1)} %bitcast.28, bf16[512,256]{1,0:T(8,128)(2,1)} %pad_maximum_fusion.kv, bf16[1024,128]{1,0:T(8,128)(2,1)} %bitcast.30, f32[1024,1]{1,0:T(8,128)} %bitcast.29, f32[8,2,512]{2,1,0:T(2,128)} %bitcast.31), custom_call_target="tpu_custom_call" | custom-call | tf_op jit(solution)/shard_map/gather/pallas_call | solution.py:481
  87.0 0.0 copy-start.2
  87.0 0.0 copy-start.3
  87.0 13.2 %experts.1 = bf16[32,4,16,2048]{3,2,1,0:T(8,128)(2,1)} custom-call(bf16[32,4,16,2048]{3,2,1,0:T(8,128)(2,1)} %bitcast.27, bf16[4,2048,256]{2,1,0:T(8,128)(2,1)} %gate_w.1, bf16[4,2048,256]{2,1,0:T(8,128)(2,1)} %up_w.1, bf16[4,2048,256]{2,1,0:T(8,128)(2,1)} %down_w.1), custom_call_target="tpu_custom_call" | custom-call | tf_op jit(solution)/shard_map/experts/pallas_call | solution.py:508
  100.2 0.0 copy-done.2
  100.3 0.0 copy-done.3
  100.3 0.7 copy.36.slots_weights
  101.0 75.6 %give_back.1 = (bf16[128,2048]{1,0:T(8,128)(2,1)}, bf16[128,2048]{1,0:T(8,128)(2,1)}) custom-call(bf16[4,8,64,2048]{3,2,1,0:T(8,128)(2,1)} %bitcast.26, bf16[4,2,128,128]{3,2,1,0:T(8,128)(2,1)} %get-tuple-element.5.att_all, bf16[1024,2048]{1,0:T(8,128)(2,1)} %mixer.1, f32[128,4]{1,0:T(8,128)} %copy.36.slots_weights), custom_call_target="tpu_custom_call" | custom-call | tf_op jit(solution)/shard_map/give_back/pallas_call | solution.py:520
  176.6 1.9 %copy.42 = bf16[128,2048]{1,0:T(8,128)(2,1)} copy(bf16[128,2048]{1,0:T(8,128)(2,1)} %get-tuple-element.16) | data formatting | bytes 1048576
  178.5 1.9 %copy.43 = bf16[128,2048]{1,0:T(8,128)(2,1)} copy(bf16[128,2048]{1,0:T(8,128)(2,1)} %get-tuple-element.17) | data formatting | bytes 1048576
  (7 shorter events, 0.1 us)
Async XLA Ops:
  0.6 9.8 %copy-start.4 = (f32[128]{0:T(128)S(1)}, f32[128]{0:T(128)}, u32[]{:S(2)}) copy-start(f32[128]{0:T(128)} %param.18) | copy-start | bytes 1540
  0.6 11.3 %copy-start = (bf16[512,128]{1,0:T(8,128)(2,1)S(1)}, bf16[512,128]{1,0:T(8,128)(2,1)}, u32[]{:S(2)}) copy-start(bf16[512,128]{1,0:T(8,128)(2,1)} %param.15) | copy-start | bytes 393220
  0.7 11.4 %copy-start.5 = (f32[128]{0:T(128)S(1)}, f32[128]{0:T(128)}, u32[]{:S(2)}) copy-start(f32[128]{0:T(128)} %param.19) | copy-start | bytes 1540
  0.7 11.6 %copy-start.1 = (bf16[512,128]{1,0:T(8,128)(2,1)S(1)}, bf16[512,128]{1,0:T(8,128)(2,1)}, u32[]{:S(2)}) copy-start(bf16[512,128]{1,0:T(8,128)(2,1)} %param.16) | copy-start | bytes 393220
  87.0 13.3 %copy-start.2 = (s32[128,2]{0,1:T(2,128)S(1)}, s32[128,2]{0,1:T(2,128)}, u32[]{:S(2)}) copy-start(s32[128,2]{0,1:T(2,128)} %param.23) | copy-start | bytes 3076
  87.0 13.3 %copy-start.3 = (f32[128,2]{0,1:T(2,128)S(1)}, f32[128,2]{0,1:T(2,128)}, u32[]{:S(2)}) copy-start(f32[128,2]{0,1:T(2,128)} %param.24) | copy-start | bytes 3076

commit v3 on v2

v3 whole, which is shorter than its diff:
```python
import functools

import jax
import jax.numpy as jnp
from jax import lax
from jax.experimental import pallas as pl
from jax.experimental.pallas import tpu as pltpu
from jax.sharding import PartitionSpec as P

CAP = 16
EPSILON = 1e-06
NEGATIVE = -1e30
MESH = pl.DeviceIdType.MESH
VMEM_LIMIT = 62 * 1024 * 1024


def rms_scale(inputs, gain):
    inputs = inputs.astype(jnp.float32)
    return inputs * lax.rsqrt(jnp.mean(inputs * inputs, axis=-1, keepdims=True) + EPSILON) * gain


def places(n_tp):
    ep, tp = lax.axis_index("ep"), lax.axis_index("tp")
    core = tp + 1 - 2 * lax.rem(tp, 2)
    across = lax.rem(tp + n_tp // 2, n_tp)
    corner = lax.rem(core + n_tp // 2, n_tp)
    return ep, tp, core, across, corner


def weights_of(count):
    digits = count.bit_length() - 1
    assert count == 1 << digits
    return [1] + [1 << (digits - number) for number in range(1, digits)]


def paired(place, slot, count):
    result = 0
    for number, weight in enumerate(weights_of(count)):
        result = result + weight * lax.rem(lax.div(place, weight) + lax.div(slot, 1 << number), 2)
    return result


def meet(n_ep, n_tp):
    ep, tp = lax.axis_index("ep"), lax.axis_index("tp")
    barrier = pltpu.get_barrier_semaphore()
    for step in range(1, n_ep):
        pl.semaphore_signal(
            barrier, inc=1, device_id=(lax.rem(ep + step, n_ep), tp), device_id_type=MESH
        )
    for step in range(1, n_tp):
        pl.semaphore_signal(
            barrier, inc=1, device_id=(ep, lax.rem(tp + step, n_tp)), device_id_type=MESH
        )
    pl.semaphore_wait(barrier, n_ep + n_tp - 2)


def remote(src, dst, send, recv, ep, tp):
    return pltpu.make_async_remote_copy(
        src_ref=src, dst_ref=dst, send_sem=send, recv_sem=recv, device_id=(ep, tp), device_id_type=MESH
    )


def layer_kernel(
    n_ep,
    n_tp,
    heads,
    outg,
    kv,
    q,
    fq,
    fk,
    slots_weights,
    gate_hbm,
    up_hbm,
    down_hbm,
    mixer_hbm,
    mixed,
    routed,
    gate_w,
    up_w,
    down_w,
    mixer,
    kvbuf,
    att,
    att_all,
    high,
    denom,
    accum,
    pieces,
    sums,
    near_own,
    near_far,
    sum_x,
    got_x,
    sum_r,
    back,
    a_send,
    a_recv,
    x_send,
    x_recv,
    c_send,
    c_recv,
    d_send,
    d_recv,
    u_send,
    k_send,
    k_recv,
    f_send,
    f_recv,
    n_send,
    n_recv,
    y_send,
    y_recv,
    r_send,
    r_recv,
    t_send,
    t_recv,
    w_sem,
    own_sem,
):
    ep, tp, core, across, corner = places(n_tp)
    rows, head_dim = kv.shape[0], q.shape[1]
    part = rows // n_tp
    scale = head_dim ** (-0.5)
    local, width, ff = gate_w.shape
    half = n_ep // 2
    level, side = lax.div(ep, 2), lax.rem(ep, 2)
    levels = n_ep // 2
    beside = ep + 1 - 2 * side
    assert local <= half
    loads = [
        pltpu.make_async_copy(src, dst, w_sem.at[number])
        for number, (src, dst) in enumerate(
            [(gate_hbm, gate_w), (up_hbm, up_w), (down_hbm, down_w), (mixer_hbm, mixer)]
        )
    ]
    meet(n_ep, n_tp)

    def up_copy(src, source):
        above = lax.rem(ep + 2, n_ep)
        return remote(src, kvbuf.at[source], u_send.at[source], k_recv.at[source], above, tp)

    def side_copy(src, source):
        return remote(src, kvbuf.at[source], k_send.at[source], k_recv.at[source], beside, tp)

    def a_copy(slot):
        other = paired(ep, slot, n_ep)
        return remote(outg.at[slot], pieces.at[tp, slot], a_send.at[slot], a_recv.at[slot], other, tp)

    def x_copy(src, owner, slot):
        return remote(src, pieces.at[owner, slot], x_send.at[slot], x_recv.at[slot], ep, across)

    def c_copy(src, owner, slot):
        return remote(src, pieces.at[owner, slot], c_send.at[slot], c_recv.at[slot], ep, core)

    def d_copy(src, owner, slot):
        return remote(src, pieces.at[owner, slot], d_send.at[slot], d_recv.at[slot], ep, core)

    def far_copy(slot):
        return remote(sums.at[corner, slot], near_far.at[slot], f_send.at[slot], f_recv.at[slot], ep, core)

    def own_copy(slot):
        return remote(sums.at[core, slot], near_own.at[slot], n_send.at[slot], n_recv.at[slot], ep, core)

    def y_copy(slot):
        return remote(sum_x.at[slot], got_x.at[slot], y_send.at[slot], y_recv.at[slot], ep, across)

    def r_copy(slot):
        other = paired(ep, slot, n_ep)
        return remote(sum_r.at[slot], back.at[slot], r_send.at[slot], r_recv.at[slot], other, tp)

    def each(first, last, act):
        def body(number, carry):
            act(number)
            return carry

        lax.fori_loop(first, last, body, 0)

    @pl.when(level + 1 < levels)
    def _():
        up_copy(kv, ep).start()

    @pl.when(side == 0)
    def _():
        side_copy(kv, ep).start()

    own = pltpu.make_async_copy(outg.at[0], pieces.at[tp, 0], own_sem)
    own.start()
    x_copy(outg.at[0], tp, 0).start()
    c_copy(outg.at[0], tp, 0).start()
    a_copy(1).start()
    for load in loads:
        load.start()
    tile = rows // 2

    def block(source, keys_ref, diagonal):
        keys = keys_ref[:, :head_dim]
        vals = keys_ref[:, head_dim:]
        for head in range(heads):
            key_gate = fk[source, head : head + 1, :]
            for piece in range(2):
                span = pl.ds(head * rows + piece * tile, tile)
                scores = lax.dot_general(
                    q[span, :], keys, (((1,), (1,)), ((), ())), preferred_element_type=jnp.float32
                )
                scores = scores * scale + fq[span, :] - key_gate
                if diagonal:
                    qpos = piece * tile + lax.broadcasted_iota(jnp.int32, scores.shape, 0)
                    kpos = lax.broadcasted_iota(jnp.int32, scores.shape, 1)
                    scores = jnp.where(kpos <= qpos, scores, NEGATIVE)
                top = jnp.max(scores, axis=1, keepdims=True)
                if diagonal:
                    newest = top
                else:
                    before = high[span, :]
                    newest = jnp.maximum(before, top)
                weights = jnp.exp(scores - newest)
                total = jnp.sum(weights, axis=1, keepdims=True)
                product = jnp.dot(
                    weights.astype(jnp.bfloat16), vals, preferred_element_type=jnp.float32
                )
                if not diagonal:
                    factor = jnp.exp(before - newest)
                    total = denom[span, :] * factor + total
                    product = accum[span, :] * factor + product
                high[span, :] = newest
                denom[span, :] = total
                accum[span, :] = product

    def spread(source):
        side_copy(kvbuf.at[source], source).start()

        @pl.when(level + 1 < levels)
        def _():
            up_copy(kvbuf.at[source], source).start()

    def relay(slot):
        x_copy(outg.at[0], across, slot).wait_recv()
        d_copy(pieces.at[across, slot], across, slot).start()

    @pl.when(level > 0)
    def _():
        side_copy(kv, ep - 2).wait_recv()
        spread(ep - 2)

    each(2, n_ep, lambda slot: a_copy(slot).start())
    block(ep, kv, True)

    @pl.when(side == 1)
    def _():
        side_copy(kv, ep - 1).wait_recv()
        block(ep - 1, kvbuf.at[ep - 1], False)

    def landed(slot):
        c_copy(outg.at[0], core, slot).wait_recv()
        d_copy(outg.at[0], corner, slot).wait_recv()

    def expert(number, begin):
        own_rows = pl.ds(pl.multiple_of(number * CAP, CAP), CAP)
        taken = pieces[:, begin : begin + half, own_rows, :].reshape(n_tp * half * CAP, width)
        gate = jnp.dot(taken, gate_w[number], preferred_element_type=jnp.float32)
        upward = jnp.dot(taken, up_w[number], preferred_element_type=jnp.float32)
        hidden = (gate / (1.0 + jnp.exp(-gate)) * upward).astype(jnp.bfloat16)
        columns = min(width, 512)
        for begin_column in range(0, width, columns):
            lanes = slice(begin_column, begin_column + columns)
            result = lax.dot_general(
                hidden,
                down_w[number, lanes, :],
                (((1,), (1,)), ((), ())),
                preferred_element_type=jnp.float32,
            )
            sums[:, begin : begin + half, own_rows, lanes] = result.astype(jnp.bfloat16).reshape(
                n_tp, half, CAP, columns
            )

    def onward(slot):
        a_copy(slot).wait_recv()
        x_copy(pieces.at[tp, slot], tp, slot).start()
        c_copy(pieces.at[tp, slot], tp, slot).start()

        below = level - lax.div(slot + 1, 2)
        turned = lax.rem(slot + 1, 2)
        lower = 2 * below + lax.rem(side + turned, 2)

        @pl.when(below >= 0)
        def _():
            @pl.when(slot > 1)
            def _():
                side_copy(kv, lower).wait_recv()

                @pl.when(turned == 0)
                def _():
                    spread(lower)

            block(lower, kvbuf.at[lower], False)

        relay(slot - 1)

    each(1, half, onward)

    def onward_and_expert(slot):
        onward(slot)

        @pl.when(slot == half)
        def _():
            own.wait()
            for load in loads:
                load.wait()
            each(0, half, landed)

        @pl.when(slot - half < local)
        def _():
            expert(slot - half, 0)

    each(half, n_ep, onward_and_expert)
    relay(n_ep - 1)

    def hand_over(begin):
        each(0, half, lambda step: far_copy(begin + half - 1 - step).start())
        each(0, half, lambda step: own_copy(begin + half - 1 - step).start())

        def add(step):
            slot = begin + half - 1 - step
            far_copy(slot).wait_recv()
            sum_x[slot] = (
                sums[across, slot].astype(jnp.float32) + near_far[slot].astype(jnp.float32)
            ).astype(jnp.bfloat16)
            y_copy(slot).start()

        each(0, half, add)

    def total_of(slot):
        own_copy(slot).wait_recv()
        y_copy(slot).wait_recv()
        return (
            sums[tp, slot].astype(jnp.float32)
            + near_own[slot].astype(jnp.float32)
            + got_x[slot].astype(jnp.float32)
        ).astype(jnp.bfloat16)

    def send_back(slot):
        sum_r[slot] = total_of(slot)
        r_copy(slot).start()

    hand_over(0)
    for head in range(heads):
        span = pl.ds(head * rows, rows)
        result = (accum[span, :] / denom[span, :]).astype(jnp.bfloat16)
        for owner in range(n_tp):
            att[owner, head] = result[owner * part : (owner + 1) * part]

    def t_copy(source, step):
        dest = lax.rem(tp + step, n_tp)
        return remote(att.at[dest], att_all.at[source], t_send.at[step], t_recv.at[source], ep, dest)

    for step in range(1, n_tp):
        t_copy(tp, step).start()
    att_all[tp] = att[tp]

    each(half, n_ep, landed)
    each(0, local, lambda number: expert(number, half))
    hand_over(half)

    each(1, half, lambda step: send_back(half - step))
    back[0] = total_of(0)

    for step in range(1, n_tp):
        t_copy(lax.rem(tp - step + n_tp, n_tp), step).wait()
    total = None
    for source in range(n_tp):
        for head in range(heads):
            number = source * heads + head
            term = jnp.dot(
                att_all[source, head],
                mixer[number * head_dim : (number + 1) * head_dim, :],
                preferred_element_type=jnp.float32,
            )
            total = term if total is None else total + term
    mixed[...] = total.astype(jnp.bfloat16)

    each(0, half, lambda step: send_back(n_ep - 1 - step))

    def sent(slot):
        x_copy(outg.at[0], tp, slot).wait_send()
        c_copy(outg.at[0], tp, slot).wait_send()
        d_copy(outg.at[0], tp, slot).wait_send()
        far_copy(slot).wait_send()
        own_copy(slot).wait_send()
        y_copy(slot).wait_send()

    each(0, n_ep, sent)
    each(1, n_ep, lambda slot: a_copy(slot).wait_send())

    @pl.when(level + 1 < levels)
    def _():
        up_copy(kv, ep).wait_send()

    @pl.when(side == 0)
    def _():
        side_copy(kv, ep).wait_send()

    def spread_sent(k):
        source = ep - 2 * k
        side_copy(kv, source).wait_send()

        @pl.when(level + 1 < levels)
        def _():
            up_copy(kv, source).wait_send()

    each(1, level + 1, spread_sent)
    each(1, n_ep, lambda slot: r_copy(slot).wait())

    _, per, _ = back.shape
    found_rows = back[...].reshape(n_ep * per, width)
    summed = None
    top = slots_weights.shape[1] // 2
    for choice in range(top):
        lanes = lax.broadcasted_iota(jnp.int32, (mixed.shape[0], n_ep * per), 1)
        pick = jnp.where(
            lanes.astype(jnp.float32) == slots_weights[:, choice : choice + 1], 1.0, 0.0
        ).astype(jnp.bfloat16)
        found = jnp.dot(pick, found_rows, preferred_element_type=jnp.float32)
        term = found * slots_weights[:, top + choice : top + choice + 1]
        summed = term if summed is None else summed + term
    routed[...] = summed.astype(jnp.bfloat16)


def on_device(
    n_ep,
    n_tp,
    queries,
    keys,
    values,
    forget_cache,
    query_gain,
    key_gain,
    mixer_out,
    expert_input,
    norm_gain,
    routes,
    route_weights,
    w_gate,
    w_up,
    w_down,
):
    rows, head_dim = keys.shape
    heads = forget_cache.shape[0]
    ep = lax.axis_index("ep")
    local, width, ff = w_gate.shape
    experts = local * n_ep
    tokens = expert_input.shape[0]
    per = local * CAP
    part = rows // n_tp
    vmem = pl.BlockSpec(memory_space=pltpu.VMEM)
    anywhere = pl.BlockSpec(memory_space=pl.ANY)
    dma = pltpu.SemaphoreType.DMA

    normed_q = rms_scale(queries.reshape(rows, heads, head_dim), query_gain).astype(jnp.bfloat16)
    q = normed_q.transpose(1, 0, 2).reshape(heads * rows, head_dim)
    kv = jnp.concatenate([rms_scale(keys, key_gain).astype(jnp.bfloat16), values], axis=1)
    fq = lax.dynamic_slice_in_dim(forget_cache, ep * rows, rows, 1).reshape(heads * rows, 1)
    fk = forget_cache.reshape(heads, n_ep, rows).transpose(1, 0, 2)

    normed = rms_scale(expert_input, norm_gain).astype(jnp.bfloat16)
    names = jnp.arange(experts, dtype=jnp.int32)
    named = [(routes[:, k : k + 1] == names[None, :]) for k in range(routes.shape[1])]
    anyone = functools.reduce(jnp.logical_or, named).astype(jnp.bfloat16)
    at = jnp.arange(tokens, dtype=jnp.int32)
    earlier = (at[None, :] < at[:, None]).astype(jnp.bfloat16)
    prior = jnp.dot(earlier, anyone, preferred_element_type=jnp.float32)
    ranks = [jnp.sum(jnp.where(mine, prior, 0.0), axis=1).astype(jnp.int32) for mine in named]
    differ = (routes // local) ^ ep
    slot = jnp.zeros_like(routes)
    for number, weight in enumerate(weights_of(n_ep)):
        slot = slot + (1 << number) * (differ // weight % 2)
    base = slot * per + routes % local * CAP
    slots = jnp.stack([base[:, k] + rank for k, rank in enumerate(ranks)], axis=1)
    slots_weights = jnp.concatenate([slots.astype(jnp.float32), route_weights], axis=1)
    line = jnp.arange(experts * CAP, dtype=jnp.int32)[:, None]
    place = functools.reduce(
        jnp.logical_or, [line == slots[:, k][None, :] for k in range(slots.shape[1])]
    ).astype(jnp.bfloat16)
    outg = jnp.dot(place, normed, preferred_element_type=jnp.float32).astype(jnp.bfloat16)
    outg = outg.reshape(n_ep, per, width)

    buffer = pltpu.VMEM((n_ep, per, width), jnp.bfloat16)
    return pl.pallas_call(
        functools.partial(layer_kernel, n_ep, n_tp, heads),
        out_shape=(
            jax.ShapeDtypeStruct((part, width), jnp.bfloat16),
            jax.ShapeDtypeStruct((tokens, width), jnp.bfloat16),
        ),
        in_specs=[vmem] * 6 + [anywhere] * 4,
        out_specs=(vmem, vmem),
        scratch_shapes=[pltpu.VMEM(w_gate.shape, jnp.bfloat16)] * 3
        + [
            pltpu.VMEM(mixer_out.shape, jnp.bfloat16),
            pltpu.VMEM((n_ep, rows, 2 * head_dim), jnp.bfloat16),
            pltpu.VMEM((n_tp, heads, part, head_dim), jnp.bfloat16),
            pltpu.VMEM((n_tp, heads, part, head_dim), jnp.bfloat16),
            pltpu.VMEM((heads * rows, 1), jnp.float32),
            pltpu.VMEM((heads * rows, 1), jnp.float32),
            pltpu.VMEM((heads * rows, head_dim), jnp.float32),
            pltpu.VMEM((n_tp, n_ep, per, width), jnp.bfloat16),
            pltpu.VMEM((n_tp, n_ep, per, width), jnp.bfloat16),
        ]
        + [buffer] * 6
        + [dma((n_ep,))] * 19
        + [dma((n_tp,))] * 3
        + [dma],
        compiler_params=pltpu.CompilerParams(
            collective_id=0, has_side_effects=True, vmem_limit_bytes=VMEM_LIMIT
        ),
        name="layer",
    )(outg, kv, q, fq, fk, slots_weights, w_gate, w_up, w_down, mixer_out)


def solution(mesh):
    n_ep, n_tp = mesh.shape["ep"], mesh.shape["tp"]
    in_specs = (
        P("ep", "tp"),
        P("ep", "tp"),
        P("ep", "tp"),
        P("tp", None),
        P(),
        P(),
        P(),
        P(("ep", "tp"), None),
        P(),
        P(("ep", "tp"), None),
        P(("ep", "tp"), None),
        P("ep", None, "tp"),
        P("ep", None, "tp"),
        P("ep", None, "tp"),
    )
    out_specs = (P(("ep", "tp"), None), P(("ep", "tp"), None))
    return jax.shard_map(
        functools.partial(on_device, n_ep, n_tp),
        mesh=mesh,
        in_specs=in_specs,
        out_specs=out_specs,
        check_vma=False,
    )
```

time: 181 us -> 164 us (0.906)
  the two profiles are of different devices: /device:TPU:0 before, /device:TPU:16 now
where the time goes in v3:
time: 164 us; the launch traced here: 162 us
  Pallas kernels  142 us (87%)
  local copies, waits for them, and re-layouts  8.96 us (5%)
  other arithmetic  7.83 us (5%)
  matrix products  2.29 us (1%)
    pallas_call x1, Pallas kernels, on_device(): pl.pallas_call(functools.partial(layer_kernel, n_ep, n_tp, heads), out_sh...  142 us
    unnamed x11, local copies, waits for them, and re-layouts  5.5 us

profile of v3, /device:TPU:16, one launch (start us, length us, event | category | flops | bytes accessed | tf_op | source)
XLA Modules:
  0.0 162.3 jit_solution(1297141234089240246)
XLA Ops:
  0.6 0.0 copy-start
  0.6 0.0 copy-start.1
  0.7 0.0 copy-start.2
  0.7 0.8 fusion.24
  1.4 1.2 fusion
  2.7 0.8 slice_bitcast_fusion.1
  3.4 0.2 select_reduce_fusion.1
  3.6 0.7 pad_maximum_fusion.1
  4.3 1.0 fusion.6
  5.4 0.7 dynamic-slice_bitcast_fusion
  6.1 0.7 copy.46.slots_weights
  6.8 1.0 fusion.8
  7.9 1.6 %pad_maximum_fusion.kv = bf16[512,256]{1,0:T(8,128)(2,1)} fusion(bf16[512,128]{1,0:T(8,128)(2,1)} %param.16, bf16[512,128]{1,0:T(8,128)(2,1)S(1)} %fusion.8), kind=kLoop, calls=%fused_computation.17 | loop fusion | flops 524288 | bytes 524288 | tf_op jit(solution)/shard_map/concatenate | solution.py:461
  9.5 1.0 copy.48
  10.5 1.2 reshape.82
  11.7 0.6 multiply_reduce_fusion
  12.4 0.0 copy-done.2
  12.4 0.7 fusion.9
  13.2 0.8 copy.44
  13.9 0.0 copy-done
  13.9 0.0 copy-done.1
  13.9 2.1 %convolution_convert_fusion = bf16[512,2048]{1,0:T(8,128)(2,1)} fusion(bf16[128,2048]{1,0:T(8,128)(2,1)S(1)} %copy-done, f32[2048]{0:T(1024)S(1)} %copy-done.1, f32[128]{0:T(128)S(1)} %add_rsqrt_fusion.2, s32[128]{0:T(128)S(1)} %get-tuple-element.7, s32[128]{0:T(128)S(1)} %get-tuple-element.6), kind=kOutput, calls=%fused_computation | convolution fusion | flops 270729216 | bytes 2631168 | tf_op jit(solution)/shard_map/dot_general | solution.py:484
  16.1 142.4 %layer.1 = (bf16[128,2048]{1,0:T(8,128)(2,1)}, bf16[128,2048]{1,0:T(8,128)(2,1)}) custom-call(bf16[8,64,2048]{2,1,0:T(8,128)(2,1)} %bitcast.24, bf16[512,256]{1,0:T(8,128)(2,1)} %pad_maximum_fusion.kv, bf16[1024,128]{1,0:T(8,128)(2,1)} %bitcast.26, f32[1024,1]{1,0:T(8,128)} %bitcast.25, f32[8,2,512]{2,1,0:T(2,128)} %bitcast.27, ...), custom_call_target="tpu_custom_call" | custom-call | tf_op jit(solution)/shard_map/layer/pallas_call | solution.py:488
  158.5 1.9 %copy.52 = bf16[128,2048]{1,0:T(8,128)(2,1)} copy(bf16[128,2048]{1,0:T(8,128)(2,1)} %get-tuple-element.12) | data formatting | bytes 1048576
  160.4 1.9 %copy.53 = bf16[128,2048]{1,0:T(8,128)(2,1)} copy(bf16[128,2048]{1,0:T(8,128)(2,1)} %get-tuple-element.13) | data formatting | bytes 1048576
  (7 shorter events, 0.1 us)
Async XLA Ops:
  0.6 13.3 %copy-start = (bf16[128,2048]{1,0:T(8,128)(2,1)S(1)}, bf16[128,2048]{1,0:T(8,128)(2,1)}, u32[]{:S(2)}) copy-start(bf16[128,2048]{1,0:T(8,128)(2,1)} %param.21) | copy-start | bytes 1572868
  0.6 13.3 %copy-start.1 = (f32[2048]{0:T(1024)S(1)}, f32[2048]{0:T(1024)}, u32[]{:S(2)}) copy-start(f32[2048]{0:T(1024)} %param.22) | copy-start | bytes 24580
  0.7 11.8 %copy-start.2 = (f32[128]{0:T(128)S(1)}, f32[128]{0:T(128)}, u32[]{:S(2)}) copy-start(f32[128]{0:T(128)} %param.18) | copy-start | bytes 1540

commit v4 on v3

--- a/solution.py
+++ b/solution.py
@@ -299,23 +299,6 @@
 
     each(1, half, onward)
 
-    def onward_and_expert(slot):
-        onward(slot)
-
-        @pl.when(slot == half)
-        def _():
-            own.wait()
-            for load in loads:
-                load.wait()
-            each(0, half, landed)
-
-        @pl.when(slot - half < local)
-        def _():
-            expert(slot - half, 0)
-
-    each(half, n_ep, onward_and_expert)
-    relay(n_ep - 1)
-
     def hand_over(begin):
         each(0, half, lambda step: far_copy(begin + half - 1 - step).start())
         each(0, half, lambda step: own_copy(begin + half - 1 - step).start())
@@ -343,7 +326,23 @@
         sum_r[slot] = total_of(slot)
         r_copy(slot).start()
 
-    hand_over(0)
+    def onward_and_expert(slot):
+        onward(slot)
+
+        @pl.when(slot == half)
+        def _():
+            own.wait()
+            for load in loads:
+                load.wait()
+            each(0, half, landed)
+            each(0, local, lambda number: expert(number, 0))
+            hand_over(0)
+
+    each(half, n_ep, onward_and_expert)
+    relay(n_ep - 1)
+
+    each(1, half, lambda step: send_back(half - step))
+    back[0] = total_of(0)
     for head in range(heads):
         span = pl.ds(head * rows, rows)
         result = (accum[span, :] / denom[span, :]).astype(jnp.bfloat16)
@@ -361,9 +360,6 @@
     each(half, n_ep, landed)
     each(0, local, lambda number: expert(number, half))
     hand_over(half)
-
-    each(1, half, lambda step: send_back(half - step))
-    back[0] = total_of(0)
 
     for step in range(1, n_tp):
         t_copy(lax.rem(tp - step + n_tp, n_tp), step).wait()

time: 164 us -> 170 us (1.037)
  Pallas kernels: 142 us -> 149 us
    pallas_call x1, Pallas kernels: 142 us -> 149 us  [on_device(): pl.pallas_call(functools.partial(layer_kernel, n_ep, n_tp, heads), out_sh...]
where the time goes in v4:
time: 170 us; the launch traced here: 169 us
  Pallas kernels  149 us (88%)
  local copies, waits for them, and re-layouts  8.96 us (5%)
  other arithmetic  7.83 us (5%)
  matrix products  2.29 us (1%)
    pallas_call x1, Pallas kernels, on_device(): pl.pallas_call(functools.partial(layer_kernel, n_ep, n_tp, heads), out_sh...  149 us
    unnamed x11, local copies, waits for them, and re-layouts  5.5 us

profile of v4, /device:TPU:16, one launch (start us, length us, event | category | flops | bytes accessed | tf_op | source)
XLA Modules:
  0.0 169.2 jit_solution(17616215238869716797)
XLA Ops:
  0.6 0.0 copy-start
  0.6 0.0 copy-start.1
  0.7 0.0 copy-start.2
  0.7 0.8 fusion.24
  1.4 1.2 fusion
  2.7 0.8 slice_bitcast_fusion.1
  3.4 0.2 select_reduce_fusion.1
  3.6 0.7 pad_maximum_fusion.1
  4.3 1.0 fusion.6
  5.4 0.7 dynamic-slice_bitcast_fusion
  6.1 0.7 copy.46.slots_weights
  6.8 1.0 fusion.8
  7.9 1.6 pad_maximum_fusion.kv
  9.5 1.0 copy.48
  10.5 1.2 reshape.82
  11.7 0.6 multiply_reduce_fusion
  12.4 0.0 copy-done.2
  12.4 0.7 fusion.9
  13.2 0.8 copy.44
  13.9 0.0 copy-done
  13.9 0.0 copy-done.1
  13.9 2.1 %convolution_convert_fusion = bf16[512,2048]{1,0:T(8,128)(2,1)} fusion(bf16[128,2048]{1,0:T(8,128)(2,1)S(1)} %copy-done, f32[2048]{0:T(1024)S(1)} %copy-done.1, f32[128]{0:T(128)S(1)} %add_rsqrt_fusion.2, s32[128]{0:T(128)S(1)} %get-tuple-element.7, s32[128]{0:T(128)S(1)} %get-tuple-element.6), kind=kOutput, calls=%fused_computation | convolution fusion | flops 270729216 | bytes 2631168 | tf_op jit(solution)/shard_map/dot_general | solution.py:480
  16.1 149.3 %layer.1 = (bf16[128,2048]{1,0:T(8,128)(2,1)}, bf16[128,2048]{1,0:T(8,128)(2,1)}) custom-call(bf16[8,64,2048]{2,1,0:T(8,128)(2,1)} %bitcast.24, bf16[512,256]{1,0:T(8,128)(2,1)} %pad_maximum_fusion.kv, bf16[1024,128]{1,0:T(8,128)(2,1)} %bitcast.26, f32[1024,1]{1,0:T(8,128)} %bitcast.25, f32[8,2,512]{2,1,0:T(2,128)} %bitcast.27, ...), custom_call_target="tpu_custom_call" | custom-call | tf_op jit(solution)/shard_map/layer/pallas_call | solution.py:484
  165.4 1.9 %copy.52 = bf16[128,2048]{1,0:T(8,128)(2,1)} copy(bf16[128,2048]{1,0:T(8,128)(2,1)} %get-tuple-element.12) | data formatting | bytes 1048576
  167.3 1.9 %copy.53 = bf16[128,2048]{1,0:T(8,128)(2,1)} copy(bf16[128,2048]{1,0:T(8,128)(2,1)} %get-tuple-element.13) | data formatting | bytes 1048576
  (7 shorter events, 0.1 us)
Async XLA Ops:
  0.6 13.3 %copy-start = (bf16[128,2048]{1,0:T(8,128)(2,1)S(1)}, bf16[128,2048]{1,0:T(8,128)(2,1)}, u32[]{:S(2)}) copy-start(bf16[128,2048]{1,0:T(8,128)(2,1)} %param.21) | copy-start | bytes 1572868
  0.6 13.3 %copy-start.1 = (f32[2048]{0:T(1024)S(1)}, f32[2048]{0:T(1024)}, u32[]{:S(2)}) copy-start(f32[2048]{0:T(1024)} %param.22) | copy-start | bytes 24580
  0.7 11.8 %copy-start.2 = (f32[128]{0:T(128)S(1)}, f32[128]{0:T(128)}, u32[]{:S(2)}) copy-start(f32[128]{0:T(128)} %param.18) | copy-start | bytes 1540
